TPU v7x, 32 devices: a whole 2x2x4 slice. The times are simulated.
32 devices in a mesh: grp: 2 (over y), sp: 4 (over z), tp: 4 (over x, core).
Axes of the slice: x: 2, y: 2, z: 4, core: 2. Of those that a mesh axis runs over, the one named last changes fastest.
Arguments:
- tokens: bfloat16 [4096, 2048], P(('grp', 'sp', 'tp')), parts along dimension 0, may hold values from -6 to 6
- norm_gain: bfloat16 [2048], replicated, may hold values from 0.099609375 to 1.8984375
- conv_outer_weight: bfloat16 [2048, 1024], P('sp', 'tp'), may hold values from -0.125 to 0.125
- conv_inner_weight: bfloat16 [2048, 1024], P('sp', 'tp'), may hold values from -0.125 to 0.125
- conv_input_weight: bfloat16 [2048, 1024], P('sp', 'tp'), may hold values from -0.125 to 0.125
- query_matrix: bfloat16 [2048, 1024], P('sp', 'tp'), may hold values from -0.125 to 0.125
- key_weight: bfloat16 [2048, 1024], P('sp', 'tp'), may hold values from -0.125 to 0.125
- value_weight: bfloat16 [2048, 1024], P('sp', 'tp'), may hold values from -0.125 to 0.125
- gate_weight: bfloat16 [2048, 1024], P('sp', 'tp'), may hold values from -0.125 to 0.125
- conv_taps: bfloat16 [3, 1024], P(None, 'tp'), may hold values from -3.5 to 3.5
- conv_out_weight: bfloat16 [1024, 2048], P('tp', 'sp'), may hold values from -0.125 to 0.125
- ret_out_weight: bfloat16 [1024, 2048], P('tp', 'sp'), may hold values from -0.125 to 0.125
- log_decay: float32 [4096, 8], P(('grp', 'sp'), 'tp'), parts along dimension 0, may hold values from -0.75 to 0
Outputs:
- mixed: bfloat16 [4096, 2048], P(('grp', 'sp', 'tp')), parts along dimension 0
There are 2 independent parts, one for each index of `grp`. A program takes and returns all parts, laid end to end along the dimension named above; an argument that names none is the same for every part. Nothing has to cross between parts.
All inputs are finite; a program needn't handle non-finite values.
Results may differ from a plain program's by a relative error of at most 0.025.
Values may be sent and summed in bfloat16 or wider, within the bound.
A program may use at most 64 MiB of HBM per device.

v0:
```python
import jax
import jax.numpy as jnp
from jax import lax
from jax.sharding import PartitionSpec as P

HEAD = 128
CONV_K = 3
BLOCK = 128
EPSILON = 1e-06
ROTARY_BASE = 10000.0
HIGHEST_PRECISION = lax.Precision.HIGHEST


def prefix_2(x, axis, join, neutral):
    place = lax.axis_index(axis)
    gathered = jax.tree.map(
        lambda a, kind: lax.all_gather(a.astype(kind), axis), x, (jnp.bfloat16, jnp.bfloat16)
    )
    state = jax.tree.map(lambda a, e: jnp.zeros_like(a) + jnp.asarray(e, a.dtype), x, neutral)

    def one(turn, state):
        return join(
            state,
            jax.tree.map(
                lambda a, own: lax.dynamic_index_in_dim(a, turn, 0, False).astype(own.dtype),
                gathered,
                x,
            ),
        )

    return lax.fori_loop(0, place, one, state)


def shifted(x, axis, by):
    count = lax.axis_size(axis)
    pairs = [(i, i + by) for i in range(count) if 0 <= i + by < count]
    return lax.ppermute(x, axis, pairs)


def rotate(head_data, positions):
    half_width = head_data.shape[-1] // 2
    inv_freq = ROTARY_BASE ** (-jnp.arange(half_width, dtype=jnp.float32) / half_width)
    angles = positions[:, None] * inv_freq[None, :]
    cosine = jnp.cos(angles)[:, None, :]
    sine_part = jnp.sin(angles)[:, None, :]
    first_half = head_data[..., :half_width]
    second_half = head_data[..., half_width:]
    return jnp.concatenate(
        [
            first_half * cosine - second_half * sine_part,
            second_half * cosine + first_half * sine_part,
        ],
        axis=-1,
    )


def head_norm(head_data):
    return head_data * lax.rsqrt(jnp.mean(head_data * head_data, axis=-1, keepdims=True) + EPSILON)


def combine_states(earlier, later):
    return (earlier[0] * later[0], later[0][:, None, None] * earlier[1] + later[1])


def body(
    tokens,
    norm_gain,
    conv_outer_weight,
    conv_inner_weight,
    conv_input_weight,
    query_matrix,
    key_weight,
    value_weight,
    gate_weight,
    conv_taps,
    conv_out_weight,
    ret_out_weight,
    log_decay,
):
    values32 = tokens.astype(jnp.float32)
    normed = (
        values32
        * lax.rsqrt(jnp.mean(values32 * values32, axis=-1, keepdims=True) + EPSILON)
        * norm_gain.astype(jnp.float32)
    ).astype(jnp.bfloat16)
    gathered = lax.all_gather(normed, "tp", axis=0, tiled=True)
    row_total = gathered.shape[0]
    whole = (
        lax.all_gather(conv_outer_weight, "sp", axis=0, tiled=True),
        lax.all_gather(conv_inner_weight, "sp", axis=0, tiled=True),
        lax.all_gather(conv_input_weight, "sp", axis=0, tiled=True),
        lax.all_gather(query_matrix, "sp", axis=0, tiled=True),
        lax.all_gather(key_weight, "sp", axis=0, tiled=True),
        lax.all_gather(value_weight, "sp", axis=0, tiled=True),
        lax.all_gather(gate_weight, "sp", axis=0, tiled=True),
    )
    projected = tuple(
        (
            jnp.dot(gathered, weight, preferred_element_type=jnp.float32).astype(jnp.bfloat16)
            for weight in whole
        )
    )
    conv_outer, conv_inner, conv_input, query_proj, key_proj, value_proj, gate_proj = projected
    heads_here = query_proj.shape[1] // HEAD
    offset = (lax.axis_index("sp") * row_total).astype(jnp.float32)
    positions = offset + jnp.arange(row_total, dtype=jnp.float32)
    head_shape = (row_total, heads_here, HEAD)
    queries = rotate(query_proj.astype(jnp.float32).reshape(head_shape), positions)
    keys_rot = rotate(key_proj.astype(jnp.float32).reshape(head_shape), positions) * HEAD ** (-0.5)
    head_values = value_proj.astype(jnp.float32).reshape(head_shape)
    block_count = row_total // BLOCK
    block_shape = (block_count, BLOCK, heads_here, HEAD)
    query_blocks = queries.reshape(block_shape)
    key_blocks = keys_rot.reshape(block_shape)
    value_blocks = head_values.reshape(block_shape)
    log_blocks = log_decay.reshape(block_count, BLOCK, heads_here)
    offsets = jnp.arange(BLOCK, dtype=jnp.int32)
    causal_mask = offsets[:, None] >= offsets[None, :]
    lower_ones = causal_mask.astype(jnp.float32)
    cumulative = jnp.einsum("ij,njh->nih", lower_ones, log_blocks, precision=HIGHEST_PRECISION)
    block_end = cumulative[:, -1, :]
    mixed_in = conv_inner.astype(jnp.float32) * conv_input.astype(jnp.float32)
    rim = shifted(mixed_in[row_total - (CONV_K - 1) :], "sp", 1)
    extended = jnp.concatenate([rim, mixed_in], axis=0)
    taps = conv_taps.astype(jnp.float32)
    conv_out = jnp.zeros(mixed_in.shape, jnp.float32)
    for tap_index in range(CONV_K):
        conv_out = conv_out + taps[tap_index][None, :] * extended[tap_index : tap_index + row_total]
    conv_branch = (conv_outer.astype(jnp.float32) * conv_out).astype(jnp.bfloat16)
    weights = jnp.exp(block_end[:, None, :] - cumulative)
    increments = jnp.einsum(
        "njh,njhd,njhe->nhde", weights, key_blocks, value_blocks, precision=HIGHEST_PRECISION
    )

    def carry_on(carried, pieces):
        block_decay, increment = pieces
        return (block_decay[:, None, None] * carried + increment, carried)

    start_state = jnp.zeros((heads_here, HEAD, HEAD), jnp.float32)
    local_end, local_before = lax.scan(carry_on, start_state, (jnp.exp(block_end), increments))
    device_decay = jnp.exp(jnp.sum(block_end, axis=0))
    incoming = prefix_2(
        (device_decay, local_end),
        "sp",
        combine_states,
        (jnp.ones_like(device_decay), jnp.zeros_like(local_end)),
    )
    local_before, incoming_state = (local_before, incoming[1])
    spread = cumulative[:, :, None, :] - cumulative[:, None, :, :]
    grid_mask = causal_mask[None, :, :, None]
    decay_grid = jnp.where(grid_mask, jnp.exp(jnp.where(grid_mask, spread, 0.0)), 0.0)
    scores = (
        jnp.einsum("nihd,njhd->nijh", query_blocks, key_blocks, precision=HIGHEST_PRECISION)
        * decay_grid
    )
    within = jnp.einsum("nijh,njhe->nihe", scores, value_blocks, precision=HIGHEST_PRECISION)
    prefix = jnp.exp(jnp.cumsum(block_end, axis=0) - block_end)
    before = local_before + prefix[:, :, None, None] * incoming_state[None]
    across = jnp.einsum("nihd,nhde->nihe", query_blocks, before, precision=HIGHEST_PRECISION)
    across = across * jnp.exp(cumulative)[..., None]
    retained = (within + across).reshape(head_shape)
    ret_branch = (
        head_norm(retained).reshape(row_total, heads_here * HEAD)
        * jax.nn.silu(gate_proj.astype(jnp.float32))
    ).astype(jnp.bfloat16)
    conv_rows_weight, ret_rows_weight = (
        lax.all_gather(conv_out_weight, "sp", axis=1, tiled=True),
        lax.all_gather(ret_out_weight, "sp", axis=1, tiled=True),
    )
    return lax.psum_scatter(
        (
            jnp.dot(conv_branch, conv_rows_weight, preferred_element_type=jnp.float32)
            + jnp.dot(ret_branch, ret_rows_weight, preferred_element_type=jnp.float32)
        ).astype(jnp.bfloat16),
        "tp",
        scatter_dimension=0,
        tiled=True,
    )


def solution(mesh):
    placed = (
        P(("grp", "sp", "tp"), None),
        P(),
        P("sp", "tp"),
        P("sp", "tp"),
        P("sp", "tp"),
        P("sp", "tp"),
        P("sp", "tp"),
        P("sp", "tp"),
        P("sp", "tp"),
        P(None, "tp"),
        P("tp", "sp"),
        P("tp", "sp"),
        P(("grp", "sp"), "tp"),
    )
    return jax.shard_map(
        body, mesh=mesh, in_specs=placed, out_specs=P(("grp", "sp", "tp"), None), check_vma=False
    )
```

profile of v0, /device:TPU:0, one launch (start us, length us, event | category | flops | bytes accessed | tf_op | source)
XLA Modules:
  0.0 343.9 jit_solution(5092971589011308150)
XLA Ops:
  8.0 1.3 fusion.9
  9.3 2.0 fusion.11
  20.9 14.0 %all-reduce = bf16[8]{0:T(256)(128)(2,1)S(1)} all-reduce(bf16[8]{0:T(256)(128)(2,1)S(1)} %dynamic-update-slice), channel_id=2, replica_groups=mesh['grp'=2,'sp'=4,'tp'=4] {'sp'}, use_global_device_ids=true, to_apply=%add | all-reduce | flops 8 | bytes 32
  37.4 1.8 multiply_cosine_fusion
  39.9 23.6 %all-gather.13.cloned.1.call-done = bf16[512,2048]{1,0:T(8,128)(2,1)} async-done(((bf16[128,2048]{1,0:T(8,128)(2,1)}), bf16[512,2048]{1,0:T(8,128)(2,1)}) %all-gather.13.cloned.1.call-update) | async-done | bytes 2097168 | tf_op jit(solution)/shard_map/all_gather | solution.py:86
  63.5 2.6 convolution_convert_fusion.2
  66.2 1.0 copy.95
  67.2 1.0 copy.96
  68.2 24.9 %all-gather.27.cloned.1.call-done = bf16[2048,256]{1,0:T(8,128)(2,1)} async-done(((bf16[512,256]{1,0:T(8,128)(2,1)}), bf16[2048,256]{1,0:T(8,128)(2,1)}) %all-gather.27.cloned.1.call-update) | async-done | bytes 1048592 | tf_op jit(solution)/shard_map/all_gather | solution.py:92
  93.1 2.0 convolution_convert_fusion.1
  95.1 1.0 copy.97
  96.1 1.0 copy.98
  97.1 24.8 %all-gather.23.cloned.1.call-done = bf16[2048,256]{1,0:T(8,128)(2,1)} async-done(((bf16[512,256]{1,0:T(8,128)(2,1)}), bf16[2048,256]{1,0:T(8,128)(2,1)}) %all-gather.23.cloned.1.call-update) | async-done | bytes 1048592 | tf_op jit(solution)/shard_map/all_gather | solution.py:94
  121.9 1.9 convolution_convert_fusion.3
  123.9 2.9 multiply_subtract_fusion
  126.8 1.7 fusion.23
  128.5 9.4 %while.26 = (s32[]{:T(128)}, f32[2,128,128]{2,1,0:T(8,128)S(1)}, f32[4,2,128,128]{3,2,1,0:T(8,128)}, f32[4,2]{1,0:T(4,128)}, f32[4,2,128,128]{3,2,1,0:T(8,128)}, /*index=5*/s32[]{:T(128)}, s32[]{:T(128)}) while((s32[]{:T(128)}, f32[2,128,128]{2,1,0:T(8,128)S(1)}, f32[4,2,128,128]{3,2,1,0:T(8,128)}, f32[4,2]{1,0:T(4,128)}, ...), condition=%wide.region_2.3_spmd.clone, body=%wide.region_1.2_spmd.clone.sunk | while | flops 131075 | bytes 655992 | solution.py:140
  137.9 17.1 %all-gather.1 = bf16[8,128,128]{2,1,0:T(8,128)(2,1)} all-gather(bf16[2,128,128]{2,1,0:T(8,128)(2,1)S(1)} %convert_element_type.112), channel_id=3, replica_groups=mesh['grp'=2,'sp'=4,'tp'=4] {'sp'}, dimensions={0}, use_global_device_ids=true | all-gather | bytes 327680 | tf_op jit(solution)/shard_map/all_gather | solution.py:17
  155.0 2.7 fusion.7
  157.7 26.0 %all-gather.17.cloned.1.call-done = bf16[2048,256]{1,0:T(8,128)(2,1)} async-done(((bf16[512,256]{1,0:T(8,128)(2,1)}), bf16[2048,256]{1,0:T(8,128)(2,1)}) %all-gather.17.cloned.1.call-update) | async-done | bytes 1048592 | tf_op jit(solution)/shard_map/all_gather | solution.py:90
  183.7 2.2 fusion.6
  186.6 3.9 %collective-permute-start = (f32[2,256]{1,0:T(2,128)}, f32[2,256]{1,0:T(2,128)}, u32[]{:S(2)}, u32[]{:S(2)}) collective-permute-start(f32[2,256]{1,0:T(2,128)} %slice.45), channel_id=1, source_target_pairs={{0,4},{4,8},{8,12},{1,5},{5,9},{9,13},{2,6},{6,10},{10,14},{3,7},{... | collective-permute-start | bytes 6152 | tf_op jit(solution)/shard_map/ppermute | solution.py:37
  190.7 1.3 fusion.3
  192.5 1.9 multiply_reduce_fusion
  194.5 1.3 copy.85
  195.8 16.9 %all-gather.15.cloned.1.call-done = bf16[2048,256]{1,0:T(8,128)(2,1)} async-done(((bf16[512,256]{1,0:T(8,128)(2,1)}), bf16[2048,256]{1,0:T(8,128)(2,1)}) %all-gather.15.cloned.1.call-update) | async-done | bytes 1048592 | tf_op jit(solution)/shard_map/all_gather | solution.py:89
  212.7 29.0 %all-gather.21.cloned.1.call-done = bf16[256,2048]{1,0:T(8,128)(2,1)} async-done(((bf16[256,512]{1,0:T(8,128)(2,1)}), bf16[256,2048]{1,0:T(8,128)(2,1)}) %all-gather.21.cloned.1.call-update) | async-done | bytes 1048592 | tf_op jit(solution)/shard_map/all_gather | solution.py:167
  241.7 5.8 %fusion.30 = f32[512,2048]{1,0:T(8,128)} fusion(bf16[256,2048]{1,0:T(8,128)(2,1)} %all-gather.21.cloned.1.call-done, f32[2,256]{1,0:T(2,128)} %collective-permute-done, f32[512,256]{1,0:T(8,128)S(1)} %copy-done.2, bf16[512,2048]{1,0:T(8,128)(2,1)S(1)} %copy-done, bf16[2048,256]{1,0:T(8,128)(2,1)} %all-gather.15.cloned.1.call-done, f32[256]{0:T(256)S(1)} %bitcast.101, ...), kind=kOutput, calls=%fused_computation.62 | convolution fusion | flops 1075183616 | bytes 8918016 | tf_op jit(solution)/shard_map/dot_general | solution.py:172
  247.5 23.1 %all-gather.29.cloned.1.call-done = bf16[2048,256]{1,0:T(8,128)(2,1)} async-done(((bf16[512,256]{1,0:T(8,128)(2,1)}), bf16[2048,256]{1,0:T(8,128)(2,1)}) %all-gather.29.cloned.1.call-update) | async-done | bytes 1048592 | tf_op jit(solution)/shard_map/all_gather | solution.py:95
  270.6 28.8 %all-gather.31.cloned.1.call-done = bf16[256,2048]{1,0:T(8,128)(2,1)} async-done(((bf16[256,512]{1,0:T(8,128)(2,1)}), bf16[256,2048]{1,0:T(8,128)(2,1)}) %all-gather.31.cloned.1.call-update) | async-done | bytes 1048592 | tf_op jit(solution)/shard_map/all_gather | solution.py:168
  300.0 6.5 %add_convert_fusion = bf16[512,2048]{1,0:T(8,128)(2,1)} fusion(f32[512,2048]{1,0:T(8,128)} %fusion.30, bf16[256,2048]{1,0:T(8,128)(2,1)} %all-gather.31.cloned.1.call-done, f32[64,8,2,128]{3,2,1,0:T(2,128)S(1)} %bitcast.95, f32[64,8,2,128]{3,2,1,0:T(2,128)S(1)} %bitcast.94, bf16[512,2048]{1,0:T(8,128)(2,1)S(1)} %copy-done, ...), kind=kOutput, calls=%fused_computation.6 | convolution fusion | flops 1077018624 | bytes 11534336 | tf_op jit(solution)/shard_map/dot_general | solution.py:173
  306.6 30.7 %reduce-scatter.2.cloned.1.call-done = bf16[128,2048]{1,0:T(8,128)(2,1)} async-done(((bf16[512,2048]{1,0:T(8,128)(2,1)}), bf16[128,2048]{1,0:T(8,128)(2,1)}) %reduce-scatter.2.cloned.1.call-update) | async-done | bytes 524304 | tf_op jit(solution)/shard_map/reduce_scatter | solution.py:170
  (106 shorter events, 25.1 us)
Async XLA Ops:
  6.5 33.4 %all-gather.25.cloned.1.call-start = ((), (), s32[]{:S(2)}) async-start(), calls=%async_computation.7 | async-start | bytes 1310720 | tf_op jit(solution)/shard_map/all_gather | solution.py:93
  7.3 56.2 %all-gather.13.cloned.1.call-start = ((), (), s32[]{:S(2)}) async-start(), calls=%async_computation.1 | async-start | bytes 2621440 | tf_op jit(solution)/shard_map/all_gather | solution.py:86
  8.0 8.7 %copy-start.14 = (f32[512,2]{0,1:T(2,128)S(1)}, f32[512,2]{0,1:T(2,128)}, u32[]{:S(2)}) copy-start(f32[512,2]{0,1:T(2,128)} %param.29) | copy-start | bytes 12292
  8.0 10.7 %copy-start.15 = (u32[32]{0:T(128)S(1)}, u32[32]{0:T(128)}, u32[]{:S(2)}) copy-start(u32[32]{0:T(128)} %constant.65) | copy-start | bytes 388
  8.0 28.8 %copy-start.10 = (bf16[3,256]{1,0:T(4,128)(2,1)S(1)}, bf16[3,256]{1,0:T(4,128)(2,1)}, u32[]{:S(2)}) copy-start(bf16[3,256]{1,0:T(4,128)(2,1)} %param.26) | copy-start | bytes 4612
  11.3 81.8 %all-gather.27.cloned.1.call-start = ((), (), s32[]{:S(2)}) async-start(), calls=%async_computation.8 | async-start | bytes 1310720 | tf_op jit(solution)/shard_map/all_gather | solution.py:92
  12.1 109.8 %all-gather.23.cloned.1.call-start = ((), (), s32[]{:S(2)}) async-start(), calls=%async_computation.6 | async-start | bytes 1310720 | tf_op jit(solution)/shard_map/all_gather | solution.py:94
  12.6 142.4 %all-gather.19.cloned.1.call-start = ((), (), s32[]{:S(2)}) async-start(), calls=%async_computation.4 | async-start | bytes 1310720 | tf_op jit(solution)/shard_map/all_gather | solution.py:91
  13.2 170.5 %all-gather.17.cloned.1.call-start = ((), (), s32[]{:S(2)}) async-start(), calls=%async_computation.3 | async-start | bytes 1310720 | tf_op jit(solution)/shard_map/all_gather | solution.py:90
  13.8 198.9 %all-gather.15.cloned.1.call-start = ((), (), s32[]{:S(2)}) async-start(), calls=%async_computation.2 | async-start | bytes 1310720 | tf_op jit(solution)/shard_map/all_gather | solution.py:89
  14.6 227.1 %all-gather.21.cloned.1.call-start = ((), (), s32[]{:S(2)}) async-start(), calls=%async_computation.5 | async-start | bytes 1310720 | tf_op jit(solution)/shard_map/all_gather | solution.py:167
  15.3 255.3 %all-gather.29.cloned.1.call-start = ((), (), s32[]{:S(2)}) async-start(), calls=%async_computation.9 | async-start | bytes 1310720 | tf_op jit(solution)/shard_map/all_gather | solution.py:95
  16.0 283.4 %all-gather.31.cloned.1.call-start = ((), (), s32[]{:S(2)}) async-start(), calls=%async_computation.10 | async-start | bytes 1310720 | tf_op jit(solution)/shard_map/all_gather | solution.py:168
  16.6 320.7 %reduce-scatter.2.cloned.1.call-start = ((), (), s32[]{:S(2)}) async-start(), calls=%async_computation.11 | async-start | bytes 2621440 | tf_op jit(solution)/shard_map/reduce_scatter | solution.py:170
  66.1 27.0 %copy-start = (bf16[512,2048]{1,0:T(8,128)(2,1)S(1)}, bf16[512,2048]{1,0:T(8,128)(2,1)}, u32[]{:S(2)}) copy-start(bf16[512,2048]{1,0:T(8,128)(2,1)} %all-gather.13.cloned.1.call-done) | copy-start | bytes 6291460
  123.9 2.9 copy-start.8
  183.7 6.7 %copy-start.3 = (f32[512,2,64]{2,0,1:T(8,128)S(1)}, f32[512,2,64]{2,0,1:T(8,128)}, u32[]{:S(2)}) copy-start(f32[512,2,64]{2,0,1:T(8,128)} %get-tuple-element.140) | copy-start | bytes 786436
  183.7 6.7 %copy-start.4 = (f32[512,2,64]{2,0,1:T(8,128)S(1)}, f32[512,2,64]{2,0,1:T(8,128)}, u32[]{:S(2)}) copy-start(f32[512,2,64]{2,0,1:T(8,128)} %get-tuple-element.141) | copy-start | bytes 786436
  183.7 6.9 %copy-start.6 = (f32[4,128,2]{1,2,0:T(2,128)S(1)}, f32[4,128,2]{1,2,0:T(2,128)}, u32[]{:S(2)}) copy-start(f32[4,128,2]{1,2,0:T(2,128)} %copy.73) | copy-start | bytes 12292
  185.9 4.5 %copy-start.1 = (f32[512,256]{1,0:T(8,128)}, f32[512,256]{1,0:T(8,128)S(1)}, u32[]{:S(2)}) copy-start(f32[512,256]{1,0:T(8,128)S(1)} %fusion.6) | copy-start | bytes 1572868
  186.6 55.1 %collective-permute-start = (f32[2,256]{1,0:T(2,128)}, f32[2,256]{1,0:T(2,128)}, u32[]{:S(2)}, u32[]{:S(2)}) collective-permute-start(f32[2,256]{1,0:T(2,128)} %slice.45), channel_id=1, source_target_pairs={{0,4},{4,8},{8,12},{1,5},{5,9},{9,13},{2,6},{6,10},{10,14},{3,7},{... | collective-permute-start | bytes 6152 | tf_op jit(solution)/shard_map/ppermute | solution.py:37
  190.6 1.8 copy-start.5
  190.7 1.8 copy-start.7
  190.7 1.8 copy-start.9
  192.4 49.2 %copy-start.2 = (f32[512,256]{1,0:T(8,128)S(1)}, f32[512,256]{1,0:T(8,128)}, u32[]{:S(2)}) copy-start(f32[512,256]{1,0:T(8,128)} %copy-done.1) | copy-start | bytes 1572868
  192.4 49.2 %copy-start.11 = (f32[1,256]{1,0:T(1,128)S(1)}, f32[1,256]{1,0:T(1,128)}, u32[]{:S(2)}) copy-start(f32[1,256]{1,0:T(1,128)} %get-tuple-element.154) | copy-start | bytes 3076
  192.4 49.2 %copy-start.12 = (f32[1,256]{1,0:T(1,128)S(1)}, f32[1,256]{1,0:T(1,128)}, u32[]{:S(2)}) copy-start(f32[1,256]{1,0:T(1,128)} %get-tuple-element.155) | copy-start | bytes 3076
  192.4 49.2 %copy-start.13 = (f32[1,256]{1,0:T(1,128)S(1)}, f32[1,256]{1,0:T(1,128)}, u32[]{:S(2)}) copy-start(f32[1,256]{1,0:T(1,128)} %get-tuple-element.156) | copy-start | bytes 3076
Sparse Core Ops, SparseCore 0:
  8.9 30.9 all-gather.24
  41.5 21.9 all-gather.12
  65.1 27.9 all-gather.26
  94.5 27.3 all-gather.22
  123.3 31.5 all-gather.18
  156.4 27.3 all-gather.16
  185.3 27.3 all-gather.14
  214.3 27.3 all-gather.20
  243.2 27.3 all-gather.28
  272.0 27.3 all-gather.30
  306.7 30.5 reduce-scatter.1
where the time goes:
time: 345 us; the launch traced here: 344 us
  waiting for transfers between devices  234 us (68%)
  blocking collectives  31.1 us (9%)
  matrix products  29.2 us (8%)
  other arithmetic  16 us (5%)
  local copies, waits for them, and re-layouts  15 us (4%)
  between operations  14.2 us (4%)
  starting transfers between devices  4.26 us (1%)
    reduce_scatter x1, waiting for transfers between devices, body(): lax.psum_scatter((jnp.dot(conv_branch, conv_rows_weight, preferred_elemen...  30.7 us
    all_gather x1, waiting for transfers between devices, body(): lax.all_gather(conv_out_weight, 'sp', axis=1, tiled=True)  29 us
    all_gather x1, waiting for transfers between devices, body(): lax.all_gather(ret_out_weight, 'sp', axis=1, tiled=True)  28.8 us
    all_gather x1, waiting for transfers between devices, body(): lax.all_gather(conv_inner_weight, 'sp', axis=0, tiled=True)  26 us
    all_gather x1, waiting for transfers between devices, body(): lax.all_gather(query_matrix, 'sp', axis=0, tiled=True)  24.9 us
    all_gather x1, waiting for transfers between devices, body(): lax.all_gather(value_weight, 'sp', axis=0, tiled=True)  24.8 us
    all_gather x1, waiting for transfers between devices, body(): gathered = lax.all_gather(normed, 'tp', axis=0, tiled=True)  23.6 us
    all_gather x1, waiting for transfers between devices, body(): lax.all_gather(gate_weight, 'sp', axis=0, tiled=True)  23.1 us
  transfers between devices with their start and end apart: 12, of which 10 were waited for; matrix products, arithmetic and copies ran while one was open for 15% of the time, Pallas kernels for 0%

commit v1 on v0

--- a/solution.py
+++ b/solution.py
@@ -2,6 +2,7 @@
 import jax.numpy as jnp
 from jax import lax
 from jax.sharding import PartitionSpec as P
+from jax.lax import all_gather
 
 HEAD = 128
 CONV_K = 3
@@ -164,7 +165,7 @@
         * jax.nn.silu(gate_proj.astype(jnp.float32))
     ).astype(jnp.bfloat16)
     conv_rows_weight, ret_rows_weight = (
-        lax.all_gather(conv_out_weight, "sp", axis=1, tiled=True),
+        jnp.concatenate(all_gather(conv_out_weight, "sp"), 1),
         lax.all_gather(ret_out_weight, "sp", axis=1, tiled=True),
     )
     return lax.psum_scatter(

time: 345 us -> 345 us (level)
    all_gather x1, waiting for transfers between devices: 29 us -> 0.74 us  [body(): all_gather(conv_out_weight, 'sp')]
    all_gather x1, waiting for transfers between devices: 0.74 us -> 26.7 us  [body(): lax.all_gather(key_weight, 'sp', axis=0, tiled=True)]
  transfers between devices with their start and end apart: 12 -> 12, of which waited for: 10 -> 11; matrix products, arithmetic and copies ran while one was open for 15% -> 16% of each run, Pallas kernels for 0% -> 0%
where the time goes in v1:
time: 345 us; the launch traced here: 344 us
  waiting for transfers between devices  231 us (67%)
  blocking collectives  31.1 us (9%)
  matrix products  29.6 us (9%)
  local copies, waits for them, and re-layouts  18 us (5%)
  other arithmetic  15.9 us (5%)
  between operations  14.2 us (4%)
  starting transfers between devices  4.32 us (1%)
    reduce_scatter x1, waiting for transfers between devices, body(): lax.psum_scatter((jnp.dot(conv_branch, conv_rows_weight, preferred_elemen...  30.7 us
    all_gather x1, waiting for transfers between devices, body(): lax.all_gather(ret_out_weight, 'sp', axis=1, tiled=True)  28.8 us
    all_gather x1, waiting for transfers between devices, body(): lax.all_gather(key_weight, 'sp', axis=0, tiled=True)  26.7 us
    all_gather x1, waiting for transfers between devices, body(): lax.all_gather(conv_inner_weight, 'sp', axis=0, tiled=True)  26.1 us
    all_gather x1, waiting for transfers between devices, body(): lax.all_gather(value_weight, 'sp', axis=0, tiled=True)  24.8 us
    all_gather x1, waiting for transfers between devices, body(): lax.all_gather(query_matrix, 'sp', axis=0, tiled=True)  24.8 us
    all_gather x1, waiting for transfers between devices, body(): gathered = lax.all_gather(normed, 'tp', axis=0, tiled=True)  23.5 us
    all_gather x1, waiting for transfers between devices, body(): lax.all_gather(gate_weight, 'sp', axis=0, tiled=True)  22.8 us
  transfers between devices with their start and end apart: 12, of which 11 were waited for; matrix products, arithmetic and copies ran while one was open for 16% of the time, Pallas kernels for 0%

profile of v1, /device:TPU:0, one launch (start us, length us, event | category | flops | bytes accessed | tf_op | source)
XLA Modules:
  0.0 344.0 jit_solution(14169159024597653217)
XLA Ops:
  8.8 1.2 fusion.9
  10.0 2.0 fusion.11
  20.9 14.0 %all-reduce = bf16[8]{0:T(256)(128)(2,1)S(1)} all-reduce(bf16[8]{0:T(256)(128)(2,1)S(1)} %dynamic-update-slice), channel_id=3, replica_groups=mesh['grp'=2,'sp'=4,'tp'=4] {'sp'}, use_global_device_ids=true, to_apply=%add | all-reduce | flops 8 | bytes 32
  37.4 1.8 multiply_cosine_fusion
  39.9 2.3 copy.88
  42.2 26.7 %all-gather.24.cloned.1.call-done = bf16[2048,256]{1,0:T(8,128)(2,1)} async-done(((bf16[512,256]{1,0:T(8,128)(2,1)}), bf16[2048,256]{1,0:T(8,128)(2,1)}) %all-gather.24.cloned.1.call-update) | async-done | bytes 1048592 | tf_op jit(solution)/shard_map/all_gather | solution.py:94
  68.9 23.5 %all-gather.14.cloned.1.call-done = bf16[512,2048]{1,0:T(8,128)(2,1)} async-done(((bf16[128,2048]{1,0:T(8,128)(2,1)}), bf16[512,2048]{1,0:T(8,128)(2,1)}) %all-gather.14.cloned.1.call-update) | async-done | bytes 2097168 | tf_op jit(solution)/shard_map/all_gather | solution.py:87
  92.4 2.6 convolution_convert_fusion.2
  95.1 1.0 copy.121
  97.1 24.8 %all-gather.26.cloned.1.call-done = bf16[2048,256]{1,0:T(8,128)(2,1)} async-done(((bf16[512,256]{1,0:T(8,128)(2,1)}), bf16[2048,256]{1,0:T(8,128)(2,1)}) %all-gather.26.cloned.1.call-update) | async-done | bytes 1048592 | tf_op jit(solution)/shard_map/all_gather | solution.py:93
  121.8 2.0 convolution_convert_fusion.1
  123.9 1.0 copy.123
  124.9 1.0 copy.124
  125.9 24.8 %all-gather.22.cloned.1.call-done = bf16[2048,256]{1,0:T(8,128)(2,1)} async-done(((bf16[512,256]{1,0:T(8,128)(2,1)}), bf16[2048,256]{1,0:T(8,128)(2,1)}) %all-gather.22.cloned.1.call-update) | async-done | bytes 1048592 | tf_op jit(solution)/shard_map/all_gather | solution.py:95
  150.6 1.9 convolution_convert_fusion.3
  152.7 2.9 multiply_subtract_fusion
  155.5 1.7 fusion.23
  157.2 9.3 %while.26 = (s32[]{:T(128)}, f32[2,128,128]{2,1,0:T(8,128)S(1)}, f32[4,2,128,128]{3,2,1,0:T(8,128)}, f32[4,2]{1,0:T(4,128)}, f32[4,2,128,128]{3,2,1,0:T(8,128)}, /*index=5*/s32[]{:T(128)}, s32[]{:T(128)}) while((s32[]{:T(128)}, f32[2,128,128]{2,1,0:T(8,128)S(1)}, f32[4,2,128,128]{3,2,1,0:T(8,128)}, f32[4,2]{1,0:T(4,128)}, ...), condition=%wide.region_2.3_spmd.clone, body=%wide.region_1.2_spmd.clone.sunk | while | flops 131075 | bytes 655992 | solution.py:141
  166.5 17.1 %all-gather.2 = bf16[8,128,128]{2,1,0:T(8,128)(2,1)} all-gather(bf16[2,128,128]{2,1,0:T(8,128)(2,1)S(1)} %convert_element_type.112), channel_id=4, replica_groups=mesh['grp'=2,'sp'=4,'tp'=4] {'sp'}, dimensions={0}, use_global_device_ids=true | all-gather | bytes 327680 | tf_op jit(solution)/shard_map/all_gather | solution.py:18
  183.8 2.7 fusion.7
  186.5 26.1 %all-gather.18.cloned.1.call-done = bf16[2048,256]{1,0:T(8,128)(2,1)} async-done(((bf16[512,256]{1,0:T(8,128)(2,1)}), bf16[2048,256]{1,0:T(8,128)(2,1)}) %all-gather.18.cloned.1.call-update) | async-done | bytes 1048592 | tf_op jit(solution)/shard_map/all_gather | solution.py:91
  212.6 2.2 fusion.6
  215.4 3.9 %collective-permute-start = (f32[2,256]{1,0:T(2,128)}, f32[2,256]{1,0:T(2,128)}, u32[]{:S(2)}, u32[]{:S(2)}) collective-permute-start(f32[2,256]{1,0:T(2,128)} %slice.45), channel_id=1, source_target_pairs={{0,4},{4,8},{8,12},{1,5},{5,9},{9,13},{2,6},{6,10},{10,14},{3,7},{... | collective-permute-start | bytes 6152 | tf_op jit(solution)/shard_map/ppermute | solution.py:38
  219.6 1.3 fusion.3
  221.4 1.9 multiply_reduce_fusion
  223.5 2.1 copy.111
  225.6 16.0 %all-gather.16.cloned.1.call-done = bf16[2048,256]{1,0:T(8,128)(2,1)} async-done(((bf16[512,256]{1,0:T(8,128)(2,1)}), bf16[2048,256]{1,0:T(8,128)(2,1)}) %all-gather.16.cloned.1.call-update) | async-done | bytes 1048592 | tf_op jit(solution)/shard_map/all_gather | solution.py:90
  241.6 6.2 %fusion.30 = f32[512,2048]{1,0:T(8,128)} fusion(bf16[256,2048]{0,1:T(8,128)(2,1)S(1)} %bitcast.98, f32[2,256]{1,0:T(2,128)} %collective-permute-done, f32[512,256]{1,0:T(8,128)} %copy-done.2, bf16[512,2048]{1,0:T(8,128)(2,1)S(1)} %copy-done, bf16[2048,256]{1,0:T(8,128)(2,1)} %all-gather.16.cloned.1.call-done, f32[256]{0:T(256)S(1)} %bitcast.107, ...), kind=kOutput, calls=%fused_computation.62 | convolution fusion | flops 1075183616 | bytes 8918016 | tf_op jit(solution)/shard_map/dot_general | solution.py:173
  247.8 22.8 %all-gather.28.cloned.1.call-done = bf16[2048,256]{1,0:T(8,128)(2,1)} async-done(((bf16[512,256]{1,0:T(8,128)(2,1)}), bf16[2048,256]{1,0:T(8,128)(2,1)}) %all-gather.28.cloned.1.call-update) | async-done | bytes 1048592 | tf_op jit(solution)/shard_map/all_gather | solution.py:96
  270.6 28.8 %all-gather.30.cloned.1.call-done = bf16[256,2048]{1,0:T(8,128)(2,1)} async-done(((bf16[256,512]{1,0:T(8,128)(2,1)}), bf16[256,2048]{1,0:T(8,128)(2,1)}) %all-gather.30.cloned.1.call-update) | async-done | bytes 1048592 | tf_op jit(solution)/shard_map/all_gather | solution.py:169
  300.0 6.7 %add_convert_fusion = bf16[512,2048]{1,0:T(8,128)(2,1)} fusion(f32[512,2048]{1,0:T(8,128)} %fusion.30, bf16[256,2048]{1,0:T(8,128)(2,1)} %all-gather.30.cloned.1.call-done, f32[64,8,2,128]{3,2,1,0:T(2,128)S(1)} %bitcast.100, f32[64,8,2,128]{3,2,1,0:T(2,128)} %bitcast.99, bf16[512,2048]{1,0:T(8,128)(2,1)S(1)} %copy-done, ...), kind=kOutput, calls=%fused_computation.6 | convolution fusion | flops 1077018624 | bytes 11534336 | tf_op jit(solution)/shard_map/dot_general | solution.py:174
  306.7 30.7 %reduce-scatter.2.cloned.1.call-done = bf16[128,2048]{1,0:T(8,128)(2,1)} async-done(((bf16[512,2048]{1,0:T(8,128)(2,1)}), bf16[128,2048]{1,0:T(8,128)(2,1)}) %reduce-scatter.2.cloned.1.call-update) | async-done | bytes 524304 | tf_op jit(solution)/shard_map/reduce_scatter | solution.py:171
  (107 shorter events, 26.1 us)
Async XLA Ops:
  6.5 33.4 %all-gather.32.cloned.1.call-start = ((), (), s32[]{:S(2)}) async-start(), calls=%async_computation.11 | async-start | bytes 1310720 | tf_op jit(solution)/shard_map/all_gather | solution.py:168
  7.3 9.5 %copy-start.14 = (f32[512,2]{0,1:T(2,128)S(1)}, f32[512,2]{0,1:T(2,128)}, u32[]{:S(2)}) copy-start(f32[512,2]{0,1:T(2,128)} %param.29) | copy-start | bytes 12292
  7.3 61.6 %all-gather.24.cloned.1.call-start = ((), (), s32[]{:S(2)}) async-start(), calls=%async_computation.6 | async-start | bytes 1310720 | tf_op jit(solution)/shard_map/all_gather | solution.py:94
  8.0 10.7 %copy-start.15 = (u32[32]{0:T(128)S(1)}, u32[32]{0:T(128)}, u32[]{:S(2)}) copy-start(u32[32]{0:T(128)} %constant.65) | copy-start | bytes 388
  8.0 28.8 %copy-start.10 = (bf16[3,256]{1,0:T(4,128)(2,1)S(1)}, bf16[3,256]{1,0:T(4,128)(2,1)}, u32[]{:S(2)}) copy-start(bf16[3,256]{1,0:T(4,128)(2,1)} %param.26) | copy-start | bytes 4612
  8.0 84.4 %all-gather.14.cloned.1.call-start = ((), (), s32[]{:S(2)}) async-start(), calls=%async_computation.1 | async-start | bytes 2621440 | tf_op jit(solution)/shard_map/all_gather | solution.py:87
  12.1 109.8 %all-gather.26.cloned.1.call-start = ((), (), s32[]{:S(2)}) async-start(), calls=%async_computation.7 | async-start | bytes 1310720 | tf_op jit(solution)/shard_map/all_gather | solution.py:93
  12.6 138.0 %all-gather.22.cloned.1.call-start = ((), (), s32[]{:S(2)}) async-start(), calls=%async_computation.5 | async-start | bytes 1310720 | tf_op jit(solution)/shard_map/all_gather | solution.py:95
  13.2 170.5 %all-gather.20.cloned.1.call-start = ((), (), s32[]{:S(2)}) async-start(), calls=%async_computation.4 | async-start | bytes 1310720 | tf_op jit(solution)/shard_map/all_gather | solution.py:92
  13.8 198.8 %all-gather.18.cloned.1.call-start = ((), (), s32[]{:S(2)}) async-start(), calls=%async_computation.3 | async-start | bytes 1310720 | tf_op jit(solution)/shard_map/all_gather | solution.py:91
  14.6 227.0 %all-gather.16.cloned.1.call-start = ((), (), s32[]{:S(2)}) async-start(), calls=%async_computation.2 | async-start | bytes 1310720 | tf_op jit(solution)/shard_map/all_gather | solution.py:90
  15.3 255.2 %all-gather.28.cloned.1.call-start = ((), (), s32[]{:S(2)}) async-start(), calls=%async_computation.8 | async-start | bytes 1310720 | tf_op jit(solution)/shard_map/all_gather | solution.py:96
  16.0 283.3 %all-gather.30.cloned.1.call-start = ((), (), s32[]{:S(2)}) async-start(), calls=%async_computation.9 | async-start | bytes 1310720 | tf_op jit(solution)/shard_map/all_gather | solution.py:169
  16.6 320.8 %reduce-scatter.2.cloned.1.call-start = ((), (), s32[]{:S(2)}) async-start(), calls=%async_computation.10 | async-start | bytes 2621440 | tf_op jit(solution)/shard_map/reduce_scatter | solution.py:171
  95.0 26.8 %copy-start = (bf16[512,2048]{1,0:T(8,128)(2,1)S(1)}, bf16[512,2048]{1,0:T(8,128)(2,1)}, u32[]{:S(2)}) copy-start(bf16[512,2048]{1,0:T(8,128)(2,1)} %all-gather.14.cloned.1.call-done) | copy-start | bytes 6291460
  152.7 2.9 copy-start.8
  212.6 6.8 %copy-start.3 = (f32[512,2,64]{2,0,1:T(8,128)S(1)}, f32[512,2,64]{2,0,1:T(8,128)}, u32[]{:S(2)}) copy-start(f32[512,2,64]{2,0,1:T(8,128)} %get-tuple-element.145) | copy-start | bytes 786436
  212.6 6.8 %copy-start.4 = (f32[512,2,64]{2,0,1:T(8,128)S(1)}, f32[512,2,64]{2,0,1:T(8,128)}, u32[]{:S(2)}) copy-start(f32[512,2,64]{2,0,1:T(8,128)} %get-tuple-element.146) | copy-start | bytes 786436
  212.6 7.0 %copy-start.6 = (f32[4,128,2]{1,2,0:T(2,128)S(1)}, f32[4,128,2]{1,2,0:T(2,128)}, u32[]{:S(2)}) copy-start(f32[4,128,2]{1,2,0:T(2,128)} %copy.99) | copy-start | bytes 12292
  214.8 4.6 %copy-start.2 = (f32[512,256]{1,0:T(8,128)}, f32[512,256]{1,0:T(8,128)S(1)}, u32[]{:S(2)}) copy-start(f32[512,256]{1,0:T(8,128)S(1)} %fusion.6) | copy-start | bytes 1572868
  215.4 26.1 %collective-permute-start = (f32[2,256]{1,0:T(2,128)}, f32[2,256]{1,0:T(2,128)}, u32[]{:S(2)}, u32[]{:S(2)}) collective-permute-start(f32[2,256]{1,0:T(2,128)} %slice.45), channel_id=1, source_target_pairs={{0,4},{4,8},{8,12},{1,5},{5,9},{9,13},{2,6},{6,10},{10,14},{3,7},{... | collective-permute-start | bytes 6152 | tf_op jit(solution)/shard_map/ppermute | solution.py:38
  219.6 1.8 copy-start.5
  219.6 1.8 copy-start.7
  219.6 1.8 copy-start.9
  221.4 20.2 %copy-start.1 = (bf16[256,4,512]{0,2,1:T(8,128)(2,1)S(1)}, bf16[256,4,512]{0,2,1:T(8,128)(2,1)}, u32[]{:S(2)}) copy-start(bf16[256,4,512]{0,2,1:T(8,128)(2,1)} %copy.88) | copy-start | bytes 3145732
  221.4 20.2 %copy-start.11 = (f32[1,256]{1,0:T(1,128)S(1)}, f32[1,256]{1,0:T(1,128)}, u32[]{:S(2)}) copy-start(f32[1,256]{1,0:T(1,128)} %get-tuple-element.159) | copy-start | bytes 3076
  221.4 20.2 %copy-start.12 = (f32[1,256]{1,0:T(1,128)S(1)}, f32[1,256]{1,0:T(1,128)}, u32[]{:S(2)}) copy-start(f32[1,256]{1,0:T(1,128)} %get-tuple-element.160) | copy-start | bytes 3076
  221.4 20.2 %copy-start.13 = (f32[1,256]{1,0:T(1,128)S(1)}, f32[1,256]{1,0:T(1,128)}, u32[]{:S(2)}) copy-start(f32[1,256]{1,0:T(1,128)} %get-tuple-element.161) | copy-start | bytes 3076
Sparse Core Ops, SparseCore 0:
  8.9 30.9 all-gather.31
  41.5 27.3 all-gather.23
  70.4 21.9 all-gather.13
  93.8 27.9 all-gather.25
  123.3 27.3 all-gather.21
  152.1 31.6 all-gather.19
  185.3 27.2 all-gather.17
  214.2 27.3 all-gather.15
  243.2 27.3 all-gather.27
  272.0 27.3 all-gather.29
  306.8 30.5 reduce-scatter.1
